TPU v7x, 256 devices: a 4x2x16 block of a 4x16x16 slice. The times are simulated.
256 devices in a mesh: grp: 2 (over y), sp: 32 (over z, core), tp: 4 (over x).
Axes of the slice: x: 4, y: 2, z: 16, core: 2. Of those that a mesh axis runs over, the one named last changes fastest.
The devices are a block of a 4x16x16 slice.
Arguments:
- ssm_input: bfloat16 [8192, 1024], P(('grp', 'sp'), 'tp'), parts along dimension 0, may hold values from -6 to 6
- residual_in: bfloat16 [8192, 2048], P(('grp', 'sp')), parts along dimension 0, may hold values from -4 to 4
- log_step: float32 [64], P('tp'), may hold values from -6.91 to -2.3
- decay_real: float32 [64, 64], P('tp'), may hold values from -34 to 0, as said below
- freq: float32 [64, 64], P('tp'), may hold values from 0.5 to 8
- in_real: float32 [64, 64, 16], P('tp'), may hold values from -1 to 1
- in_imag: float32 [64, 64, 16], P('tp'), may hold values from -1 to 1
- out_real: float32 [64, 16, 64], P('tp'), may hold values from -0.5 to 0.5
- out_imag: float32 [64, 16, 64], P('tp'), may hold values from -0.5 to 0.5
- skip: float32 [1024], P('tp'), may hold values from -3 to 3
- w_glu: bfloat16 [1024, 1024], replicated, may hold values from -0.1875 to 0.1875
- b_glu: float32 [1024], replicated, may hold values from -3 to 3
- w_branch: bfloat16 [1024, 2048], replicated, may hold values from -0.1875 to 0.1875
- norm_gain: float32 [2048], replicated, may hold values from 0.1 to 1.9
- w_gate: bfloat16 [2048, 5632], P('sp', 'tp'), may hold values from -0.125 to 0.125
- w_up: bfloat16 [2048, 5632], P('sp', 'tp'), may hold values from -0.125 to 0.125
- w_down: bfloat16 [5632, 2048], P('tp', 'sp'), may hold values from -0.078125 to 0.078125
Outputs:
- mixed: bfloat16 [8192, 2048], P(('grp', 'sp', 'tp')), parts along dimension 0
There are 2 independent parts, one for each index of `grp`. A program takes and returns all parts, laid end to end along the dimension named above; an argument that names none is the same for every part. Nothing has to cross between parts.
Inputs may be any that keep to these rules, and one draw needn't show every extreme that they name: `decay_real`: negative in every entry.
All inputs are finite; a program needn't handle non-finite values.
Results may differ from a plain program's by a relative error of at most 0.015.
Values may be sent and summed in bfloat16 or wider, within the bound.
A program may use at most 128 MiB of HBM per device.

v0:
```python
import math
import jax
import jax.numpy as jnp
from jax import lax
from jax.sharding import Mesh
from jax.sharding import PartitionSpec as P

SP = ("sp_0", "sp_1")
GRP_SP = ("grp", "sp_0", "sp_1")
GRP_SP_TP = ("grp", "sp_0", "sp_1", "tp")
EPS = 1e-06


def sent_together(arrays, axis, dim, along):
    ends, at = ([], 0)
    for a in arrays[:-1]:
        at += a.shape[along]
        ends.append(at)
    both = jnp.concatenate(arrays, axis=along)
    return tuple(jnp.split(lax.all_gather(both, axis, axis=dim, tiled=True), ends, axis=along))


def neutral_like(shard, identity):
    return jax.tree.map(
        lambda a, e: jnp.broadcast_to(jnp.asarray(e, a.dtype), a.shape), shard, identity
    )


def all_in_one(shard, axis):
    leaves = jax.tree.leaves(shard)
    turns = sorted(range(len(leaves)), key=lambda k: -leaves[k].size)
    width = (1, *leaves[turns[0]].shape)[-1]
    lines = [
        jnp.pad(leaves[k].reshape(-1), (0, -leaves[k].size % width)).reshape(-1, width)
        for k in turns
    ]
    both, at, found = (lax.all_gather(jnp.concatenate(lines), axis), 0, {})
    for k, line in zip(turns, lines):
        piece = both[:, at : at + len(line)].reshape(len(both), -1)
        found[k] = piece[:, : leaves[k].size].reshape(-1, *leaves[k].shape)
        at += len(line)
    numbers = iter(range(len(leaves)))
    return jax.tree.map(lambda _: found[next(numbers)], shard)


def entering_2(shard, axes, combine, identity):
    before = start = neutral_like(shard, identity)
    so_far = shard
    for axis in reversed(axes):
        count, place = (lax.axis_size(axis), lax.axis_index(axis))
        pieces = all_in_one(so_far, axis)
        inside, so_far = (start, start)
        for k in range(count):
            passed = k < place
            so_far = combine(so_far, jax.tree.map(lambda part: part[k], pieces))
            inside = jax.tree.map(lambda new, old: jnp.where(passed, new, old), so_far, inside)
        before = combine(inside, before)
    return before


def sent_to_all(shard, axis):
    count = lax.axis_size(axis)
    return lax.all_to_all(
        jnp.broadcast_to(shard[None], (count, *shard.shape)), axis, 0, 0, tiled=True
    )


def in_order(pieces, dim):
    dims = list(pieces.shape[1:])
    dims[dim] *= pieces.shape[0]
    return jnp.moveaxis(pieces, 0, dim).reshape(dims)


def gather_directly(shard, axis, dim):
    pieces = sent_to_all(shard, axis)
    return in_order(pieces, dim)


def cut_along(shard, dim, count):
    dims = shard.shape
    pieces = shard.reshape(*dims[:dim], count, dims[dim] // count, *dims[dim + 1 :])
    return jnp.moveaxis(pieces, dim, 0)


def summed_on_arrival(shard, axis, dim):
    pieces = cut_along(shard, dim, lax.axis_size(axis))
    arrived = lax.all_to_all(pieces, axis, split_axis=0, concat_axis=0, tiled=True)
    return arrived.astype(jnp.float32).sum(axis=0)


def discretize(log_step, decay_real, freq, in_real, in_imag):
    step_size = jnp.exp(log_step)[:, None]
    magnitude = jnp.exp(decay_real * step_size)
    abar_re = magnitude * jnp.cos(freq * step_size)
    abar_im = magnitude * jnp.sin(freq * step_size)
    denominator = decay_real * decay_real + freq * freq
    less_re = abar_re - 1.0
    hold_re = ((less_re * decay_real + abar_im * freq) / denominator)[..., None]
    hold_im = ((abar_im * decay_real - less_re * freq) / denominator)[..., None]
    bbar_re = hold_re * in_real - hold_im * in_imag
    bbar_im = hold_re * in_imag + hold_im * in_real
    return (step_size, abar_re, abar_im, bbar_re, bbar_im)


def powers(decay_real, freq, step_size, length):
    steps_up = (jnp.arange(length, dtype=jnp.int32) + 1).astype(jnp.float32)[:, None, None]
    magnitude = jnp.exp((decay_real * step_size)[None] * steps_up)
    phase = (freq * step_size)[None] * steps_up
    return (magnitude * jnp.cos(phase), magnitude * jnp.sin(phase))


def compose(earlier, later):
    a1r, a1i, b1r, b1i = earlier
    a2r, a2i, b2r, b2i = later
    return (
        a2r * a1r - a2i * a1i,
        a2r * a1i + a2i * a1r,
        a2r * b1r - a2i * b1i + b2r,
        a2r * b1i + a2i * b1r + b2i,
    )


def local_states(inputs, decay_real, freq, step_size, bbar_re, bbar_im):
    highest = lax.Precision.DEFAULT
    tok_rows, group_count, unused = inputs.shape
    lanes = group_count * decay_real.shape[1]
    drive_re = jnp.einsum("lgm,gpm->lgp", inputs, bbar_re, precision=highest).reshape(
        tok_rows, lanes
    )
    drive_im = jnp.einsum("lgm,gpm->lgp", inputs, bbar_im, precision=highest).reshape(
        tok_rows, lanes
    )
    span = math.gcd(tok_rows, 16)
    spans = tok_rows // span
    rate = (decay_real * step_size).reshape(lanes)
    turn = (freq * step_size).reshape(lanes)
    later = jnp.arange(span, dtype=jnp.int32)[:, None]
    earlier = jnp.arange(span, dtype=jnp.int32)[None, :]
    lag = (later - earlier).astype(jnp.float32)
    causal = (later >= earlier)[..., None]
    lag_pos = jnp.maximum(lag, 0.0)[..., None]
    table_mag = jnp.exp(rate[None, None] * lag_pos)
    table_re = jnp.where(causal, table_mag * jnp.cos(turn[None, None] * lag_pos), 0.0)
    table_im = jnp.where(causal, table_mag * jnp.sin(turn[None, None] * lag_pos), 0.0)
    block_re = drive_re.reshape(spans, 1, span, lanes)
    block_im = drive_im.reshape(spans, 1, span, lanes)
    inner_re = jnp.sum(table_re[None] * block_re - table_im[None] * block_im, axis=2)
    inner_im = jnp.sum(table_re[None] * block_im + table_im[None] * block_re, axis=2)
    steps_up = (jnp.arange(span, dtype=jnp.int32) + 1).astype(jnp.float32)[:, None]
    pow_mag = jnp.exp(rate[None] * steps_up)
    pow_re = pow_mag * jnp.cos(turn[None] * steps_up)
    pow_im = pow_mag * jnp.sin(turn[None] * steps_up)
    span_re = pow_re[-1]
    span_im = pow_im[-1]

    def carry_step(entering, ends):
        next_re = span_re * entering[0] - span_im * entering[1] + ends[0]
        next_im = span_re * entering[1] + span_im * entering[0] + ends[1]
        return ((next_re, next_im), entering)

    zeros = jnp.zeros((lanes,), jnp.float32)
    unused_carry, entering = lax.scan(
        carry_step, (zeros, zeros), (inner_re[:, -1], inner_im[:, -1])
    )
    state_re = inner_re + pow_re[None] * entering[0][:, None] - pow_im[None] * entering[1][:, None]
    state_im = inner_im + pow_re[None] * entering[1][:, None] + pow_im[None] * entering[0][:, None]
    shape = (tok_rows, group_count, decay_real.shape[1])
    return (state_re.reshape(shape), state_im.reshape(shape))


def readout(state_re, state_im, out_real, out_imag, skip_mat, inputs):
    highest = lax.Precision.DEFAULT
    values = (
        jnp.einsum("lgp,gmp->lgm", state_re, out_real, precision=highest)
        - jnp.einsum("lgp,gmp->lgm", state_im, out_imag, precision=highest)
        + skip_mat[None] * inputs
    )
    values = jax.nn.gelu(values)
    return values.reshape(values.shape[0], -1).astype(jnp.bfloat16)


def row_norm(stream, norm_gain):
    scale_rows = lax.rsqrt(jnp.mean(stream * stream, axis=-1, keepdims=True) + EPS)
    return (stream * scale_rows * norm_gain).astype(jnp.bfloat16)


def per_device(
    ssm_input,
    residual_in,
    log_step,
    decay_real,
    freq,
    in_real,
    in_imag,
    out_real,
    out_imag,
    skip,
    w_glu,
    b_glu,
    w_branch,
    norm_gain,
    w_gate,
    w_up,
    w_down,
):
    tok_rows, width_local = ssm_input.shape
    group_count = log_step.shape[0]
    group_size = in_real.shape[2]
    tp_count = lax.axis_size("tp")
    tp_index = lax.axis_index("tp")
    own_rows = tok_rows // tp_count
    gate_whole, up_whole = sent_together((w_gate, w_up), SP, 0, 1)
    step_size, abar_re, abar_im, bbar_re, bbar_im = discretize(
        log_step, decay_real, freq, in_real, in_imag
    )
    pow_re, pow_im = powers(decay_real, freq, step_size, tok_rows)
    inputs = ssm_input.astype(jnp.float32).reshape(tok_rows, group_count, group_size)
    local_re, local_im = local_states(inputs, decay_real, freq, step_size, bbar_re, bbar_im)
    identity = (
        jnp.ones_like(abar_re),
        jnp.zeros_like(abar_re),
        jnp.zeros_like(abar_re),
        jnp.zeros_like(abar_re),
    )
    carried = entering_2(
        (pow_re[-1], pow_im[-1], local_re[-1], local_im[-1]), SP, compose, identity
    )
    state_re = local_re + pow_re * carried[2][None] - pow_im * carried[3][None]
    state_im = local_im + pow_re * carried[3][None] + pow_im * carried[2][None]
    mixer_out = readout(
        state_re, state_im, out_real, out_imag, skip.reshape(group_count, group_size), inputs
    )
    mixer_rows = lax.all_to_all(mixer_out, "tp", split_axis=0, concat_axis=1, tiled=True)
    glu_pre = jnp.dot(mixer_rows, w_glu, preferred_element_type=jnp.float32) + b_glu
    gated = (mixer_rows.astype(jnp.float32) * jax.nn.sigmoid(glu_pre)).astype(jnp.bfloat16)
    residual_own = lax.dynamic_slice_in_dim(residual_in, tp_index * own_rows, own_rows, 0)
    stream = residual_own.astype(jnp.float32) + jnp.dot(
        gated, w_branch, preferred_element_type=jnp.float32
    )
    normed = row_norm(stream, norm_gain)
    normed_all = gather_directly(normed, "tp", 0)
    gate_sum = jnp.dot(normed_all, gate_whole, preferred_element_type=jnp.float32)
    up_sum = jnp.dot(normed_all, up_whole, preferred_element_type=jnp.float32)
    hidden = (jax.nn.silu(gate_sum) * up_sum).astype(jnp.bfloat16)
    down_whole = lax.all_gather(w_down, SP, axis=1, tiled=True)
    summed = summed_on_arrival(
        jnp.dot(hidden, down_whole, preferred_element_type=jnp.float32).astype(jnp.bfloat16),
        "tp",
        0,
    )
    return (stream + summed).astype(jnp.bfloat16)


def solution(mesh):
    torus = Mesh(
        mesh.devices.reshape(mesh.shape["grp"], 16, 2, mesh.shape["tp"]),
        ("grp", "sp_0", "sp_1", "tp"),
    )
    in_specs = (
        P(GRP_SP, "tp"),
        P(GRP_SP, None),
        P("tp"),
        P("tp", None),
        P("tp", None),
        P("tp", None, None),
        P("tp", None, None),
        P("tp", None, None),
        P("tp", None, None),
        P("tp"),
        P(),
        P(),
        P(),
        P(),
        P(SP, "tp"),
        P(SP, "tp"),
        P("tp", SP),
    )
    out_specs = P(GRP_SP_TP, None)
    return jax.shard_map(
        per_device, mesh=torus, in_specs=in_specs, out_specs=out_specs, check_vma=False
    )
```

profile of v0, /device:TPU:33, one launch (start us, length us, event | category | flops | bytes accessed | tf_op | source)
XLA Modules:
  0.0 209.0 jit_solution(3152876637672829027)
XLA Ops:
  6.6 1.9 pad_maximum_fusion
  12.0 5.8 %fusion.19 = (f32[16,16,1024]{2,1,0:T(8,128)}, f32[16,16,1024]{2,1,0:T(8,128)}) fusion(f32[1024]{0:T(1024)S(1)} %mul.861, f32[16,16]{1,0:T(8,128)S(1)} %convert_maximum_fusion, f32[1024]{0:T(1024)S(1)} %mul.856, pred[16,16]{1,0:T(8,128)(4,1)S(1)} %iota_compare_fusion), kind=kLoop, calls=%fused_computation.33 | loop fusion | flops 1572864 | bytes 2106624 | tf_op jit(solution)/shard_map/jit(_where)/select_n | solution.py:143
  17.8 2.0 convolution_bitcast_fusion.1
  19.8 2.0 convolution_bitcast_fusion
  21.8 1.5 copy.44
  24.5 1.5 copy.45
  27.2 6.3 %add_reduce_fusion = (f32[8,16,1024]{2,1,0:T(8,128)S(1)}, f32[8,16,1024]{2,1,0:T(8,128)S(1)}) fusion(f32[8,16,1024]{2,1,0:T(8,128)} %mul.885, f32[16,16,1024]{2,1,0:T(8,128)} %get-tuple-element.125, f32[8,16,1024]{2,1,0:T(8,128)} %mul.878, f32[16,16,1024]{2,1,0:T(8,128)} %get-tuple-element.124), kind=kLoop, calls=%fused_computation.6 | loop fusion | flops 16515072 | bytes 4194304 | tf_op jit(solution)/shard_map/reduce_sum | solution.py:148
  34.0 12.5 %while.17 = (s32[]{:T(128)}, f32[1024]{0:T(1024)S(1)}, f32[1024]{0:T(1024)S(1)}, f32[8,1024]{1,0:T(8,128)S(1)}, f32[8,1024]{1,0:T(8,128)}, /*index=5*/f32[1024]{...) while((s32[]{:T(128)}, f32[1024]{0:T(1024)S(1)}, ...), condition=%wide.region_3.4_spmd.clone, body=%wide.region_2.3_spmd.clone.sunk | while | flops 10243 | bytes 90243 | solution.py:162
  34.2 1.4 dynamic_update_slice.12
  45.1 1.4 dynamic_update_slice.12
  46.5 1.9 multiply_add_fusion.1
  49.8 2.3 %sub.173 = f32[128,16,64]{2,1,0:T(8,128)} reshape(f32[8,16,1024]{2,1,0:T(8,128)} %get-tuple-element.118) | data formatting | bytes 1048576 | tf_op jit(solution)/shard_map/sub | solution.py:165
  52.9 3.9 %fusion.22 = (f32[128,16,64]{2,1,0:T(8,128)S(1)}, f32[128,16,64]{2,1,0:T(8,128)S(1)}) fusion(f32[16,64]{1,0:T(8,128)S(1)} %get-tuple-element.133, f32[128]{0:T(128)S(1)} %add_convert_fusion.1, f32[16,64]{1,0:T(8,128)S(1)} %get-tuple-element.132), kind=kLoop, calls=%fused_computation.36 | loop fusion | flops 524288 | bytes 1057280 | tf_op jit(solution)/shard_map/mul | solution.py:109
  56.8 22.0 %all-gather = f32[128,64]{1,0:T(8,128)S(1)} all-gather(f32[64,64]{1,0:T(8,128)S(1)} %pad_maximum_fusion.1), channel_id=2, replica_groups=mesh['grp'=2,'sp_0'=16,'sp_1'=2,'tp'=4] {'sp_1'}, dimensions={0}, use_global_device_ids=true | all-gather | bytes 49152 | tf_op jit(solution)/shard_map/all_gather | solution.py:37
  78.9 31.6 %all-gather.1 = f32[1024,64]{1,0:T(8,128)S(1)} all-gather(f32[64,64]{1,0:T(8,128)S(1)} %pad_maximum_fusion.2), channel_id=3, replica_groups=mesh['grp'=2,'sp_0'=16,'sp_1'=2,'tp'=4] {'sp_0'}, dimensions={0}, use_global_device_ids=true | all-gather | bytes 278528 | tf_op jit(solution)/shard_map/all_gather | solution.py:37
  110.6 6.7 %multiply_add_fusion = (bf16[128,16,64]{2,1,0:T(8,128)(2,1)S(1)}, bf16[128,16,64]{2,1,0:T(8,128)(2,1)S(1)}) fusion(f32[128,16,64]{2,1,0:T(8,128)S(1)} %add.447, f32[16,64]{1,0:T(8,128)S(1)} %add_bitcast_fusion, f32[16,64]{1,0:T(8,128)S(1)} %get-tuple-element.108, f32[16,64]{1,0:T(8,128)S(1)} %get-tuple-element.133, f32[128]{0:T(128)S(1)} %add_convert_fusion.1, ...), kind=kLoop, calls=%fused_computation.42 | loop fusion | flops 1835008 | bytes 1589760 | tf_op jit(solution)/shard_map/add | solution.py:229
  120.0 4.2 %all-to-all-start = ((bf16[4,32,256]{2,1,0:T(8,128)(2,1)}), bf16[4,32,256]{2,1,0:T(8,128)(2,1)S(1)}, u32[]{:S(2)}, u32[]{:S(2)}) async-start(bf16[4,32,256]{2,1,0:T(8,128)(2,1)} %copy.48), calls=%async_computation | async-start | bytes 131072 | tf_op jit(solution)/shard_map/all_to_all | solution.py:233
  124.2 4.5 %all-to-all-done = bf16[4,32,256]{2,1,0:T(8,128)(2,1)S(1)} async-done(((bf16[4,32,256]{2,1,0:T(8,128)(2,1)}), bf16[4,32,256]{2,1,0:T(8,128)(2,1)S(1)}, u32[]{:S(2)}, u32[]{:S(2)}) %all-to-all-start) | async-done | bytes 65568 | tf_op jit(solution)/shard_map/all_to_all | solution.py:233
  128.7 3.5 %multiply_reduce_fusion = (f32[32]{0:T(128)S(1)}, f32[32,2048]{1,0:T(8,128)S(1)}) fusion(bf16[1024,2048]{1,0:T(8,128)(2,1)} %param.31, bf16[32,1024]{1,0:T(8,128)(2,1)S(1)} %bitcast.174, bf16[1024,1024]{1,0:T(8,128)(2,1)S(1)} %copy-done, f32[1024]{0:T(1024)S(1)} %copy-done.3, bf16[128,2048]{1,0:T(8,128)(2,1)} %param.20, s32[]{:T(128)S(6)} %select_n.296), kind=kOutput, calls=%fused_computation.57 | convolution fusion | flops 201818080 | bytes 6819972 | tf_op jit(solution)/shard_map/dot_general | solution.py:237
  132.4 9.4 %all_to_all.26 = bf16[4,32,2048]{2,1,0:T(8,128)(2,1)S(1)} all-to-all(bf16[4,32,2048]{2,1,0:T(8,128)(2,1)S(1)} %broadcast_in_dim.32), channel_id=1, replica_groups=mesh['grp'=2,'sp_0'=16,'sp_1'=2,'tp'=4] {'tp'}, dimensions={0} | all-to-all | bytes 1048576 | tf_op jit(solution)/shard_map/all_to_all | solution.py:63
  141.8 4.6 %fusion.2 = f32[128,1408]{1,0:T(8,128)} fusion(bf16[128,2048]{1,0:T(8,128)(2,1)S(1)} %bitcast.167, bf16[2048,2816]{1,0:T(8,128)(2,1)} %all-gather.5.cloned.1.call-done), kind=kOutput, calls=%fused_computation.10 | convolution fusion | flops 738197504 | bytes 7012352 | tf_op jit(solution)/shard_map/dot_general | solution.py:242
  146.3 34.8 %all-gather.7.cloned.1.call-done = bf16[1408,2048]{0,1:T(8,128)(2,1)} async-done(((bf16[1408,64]{0,1:T(8,128)(2,1)}), bf16[1408,2048]{0,1:T(8,128)(2,1)}) %all-gather.7.cloned.1.call-update) | async-done | bytes 5767184 | tf_op jit(solution)/shard_map/all_gather | solution.py:245
  181.1 7.4 %convolution_convert_fusion = bf16[128,2048]{1,0:T(8,128)(2,1)S(1)} fusion(bf16[1408,2048]{0,1:T(8,128)(2,1)} %all-gather.7.cloned.1.call-done, bf16[128,2048]{1,0:T(8,128)(2,1)S(1)} %bitcast.168, bf16[2048,2816]{1,0:T(8,128)(2,1)} %all-gather.5.cloned.1.call-done, f32[128,1408]{1,0:T(8,128)} %fusion.2), kind=kOutput, calls=%fused_computation.14 | convolution fusion | flops 1477738496 | bytes 13303808 | tf_op jit(solution)/shard_map/dot_general | solution.py:247
  188.6 12.9 %all_to_all.27 = bf16[4,32,2048]{2,1,0:T(8,128)(2,1)S(1)} all-to-all(bf16[4,32,2048]{2,1,0:T(8,128)(2,1)S(1)} %bitcast.169), channel_id=1, replica_groups=mesh['grp'=2,'sp_0'=16,'sp_1'=2,'tp'=4] {'tp'}, dimensions={0} | all-to-all | bytes 1048576 | tf_op jit(solution)/shard_map/all_to_all | solution.py:87
  (95 shorter events, 21.4 us)
Async XLA Ops:
  6.5 122.1 %copy-start = (bf16[1024,1024]{1,0:T(8,128)(2,1)S(1)}, bf16[1024,1024]{1,0:T(8,128)(2,1)}, u32[]{:S(2)}) copy-start(bf16[1024,1024]{1,0:T(8,128)(2,1)} %param.29) | copy-start | bytes 6291460
  6.6 135.2 %all-gather.5.cloned.1.call-start = ((), (), s32[]{:S(2)}) async-start(), calls=%async_computation.3 | async-start | bytes 11894784 | tf_op jit(solution)/shard_map/all_gather | solution.py:20
  8.5 172.6 %all-gather.7.cloned.1.call-start = ((), (), s32[]{:S(2)}) async-start(), calls=%async_computation.4 | async-start | bytes 5947392 | tf_op jit(solution)/shard_map/all_gather | solution.py:245
  27.2 24.9 %copy-start.4 = (f32[256]{0:T(256)S(1)}, f32[256]{0:T(256)}, u32[]{:S(2)}) copy-start(f32[256]{0:T(256)} %param.28) | copy-start | bytes 3076
  46.5 70.8 %copy-start.1 = (f32[16,16,64]{2,1,0:T(8,128)S(1)}, f32[16,16,64]{2,1,0:T(8,128)}, u32[]{:S(2)}) copy-start(f32[16,16,64]{2,1,0:T(8,128)} %param.26) | copy-start | bytes 196612
  49.8 78.9 %copy-start.3 = (f32[1024]{0:T(1024)S(1)}, f32[1024]{0:T(1024)}, u32[]{:S(2)}) copy-start(f32[1024]{0:T(1024)} %param.30) | copy-start | bytes 12292
  110.6 21.7 %copy-start.2 = (f32[2048]{0:T(1024)S(1)}, f32[2048]{0:T(1024)}, u32[]{:S(2)}) copy-start(f32[2048]{0:T(1024)} %param.32) | copy-start | bytes 24580
  120.0 8.7 %all-to-all-start = ((bf16[4,32,256]{2,1,0:T(8,128)(2,1)}), bf16[4,32,256]{2,1,0:T(8,128)(2,1)S(1)}, u32[]{:S(2)}, u32[]{:S(2)}) async-start(bf16[4,32,256]{2,1,0:T(8,128)(2,1)} %copy.48), calls=%async_computation | async-start | bytes 131072 | tf_op jit(solution)/shard_map/all_to_all | solution.py:233
Sparse Core Ops, SparseCore 0:
  9.2 101.0 all-gather.4
  112.1 68.9 all-gather.6
where the time goes:
time: 210 us; the launch traced here: 209 us
  blocking collectives  75.9 us (36%)
  waiting for transfers between devices  40.1 us (19%)
  other arithmetic  28.9 us (14%)
  local copies, waits for them, and re-layouts  24.7 us (12%)
  matrix products  21.3 us (10%)
  between operations  13.7 us (7%)
  starting transfers between devices  4.27 us (2%)
    all_gather x2, blocking collectives, all_in_one(): both, at, found = (lax.all_gather(jnp.concatenate(lines), axis), 0, {})  53.6 us
    all_gather x1, waiting for transfers between devices, per_device(): down_whole = lax.all_gather(w_down, SP, axis=1, tiled=True)  34.8 us
    all_to_all x1, blocking collectives, summed_on_arrival(): lax.all_to_all(pieces, axis, split_axis=0, concat_axis=0, tiled=True)  12.9 us
    dynamic_update_slice x16, local copies, waits for them, and re-layouts, local_states(): lax.scan(carry_step, (zeros, zeros), (inner_re[:, -1], inner_im[:, -1]))  12.1 us
    all_to_all x1, blocking collectives, sent_to_all(): lax.all_to_all(jnp.broadcast_to(shard[None], (count, *shard.shape)), axis...  9.36 us
    dot_general x1, matrix products, per_device(): jnp.dot(hidden, down_whole, preferred_element_type=jnp.float32)  7.42 us
    add x1, other arithmetic, per_device(): state_im = local_im + pow_re * carried[3][None] + pow_im * carried[2][None]  6.71 us
    reduce_sum x1, other arithmetic, local_states(): jnp.sum(table_re[None] * block_im + table_im[None] * block_re, axis=2)  6.35 us
  transfers between devices with their start and end apart: 3, of which 2 were waited for; matrix products, arithmetic and copies ran while one was open for 31% of the time, Pallas kernels for 0%

commit v1 on v0

--- a/solution.py
+++ b/solution.py
@@ -242,7 +242,7 @@
     gate_sum = jnp.dot(normed_all, gate_whole, preferred_element_type=jnp.float32)
     up_sum = jnp.dot(normed_all, up_whole, preferred_element_type=jnp.float32)
     hidden = (jax.nn.silu(gate_sum) * up_sum).astype(jnp.bfloat16)
-    down_whole = lax.all_gather(w_down, SP, axis=1, tiled=True)
+    down_whole = jnp.concatenate(lax.all_gather(w_down, SP), axis=1)
     summed = summed_on_arrival(
         jnp.dot(hidden, down_whole, preferred_element_type=jnp.float32).astype(jnp.bfloat16),
         "tp",

time: 210 us -> 212 us (level)
  blocking collectives: 75.9 us -> 62.5 us
  local copies, waits for them, and re-layouts: 24.7 us -> 33.7 us
  waiting for transfers between devices: 40.1 us -> 44.5 us
  starting transfers between devices: 4.27 us -> 7.66 us
    all_gather x1, waiting for transfers between devices: 0.01 us -> 39.1 us  [sent_together(): lax.all_gather(both, axis, axis=dim, tiled=True)]
    all_gather x1, waiting for transfers between devices: 34.8 us -> 0.02 us  [per_device(): down_whole = jnp.concatenate(lax.all_gather(w_down, SP), axis=1)]
    all_to_all x1 -> x0, blocking collectives: 9.36 us -> none  [sent_to_all(): lax.all_to_all(jnp.broadcast_to(shard[None], (count, *shard.shape)), axis...]
    reshape x0 -> x1, local copies, waits for them, and re-layouts: none -> 4.45 us  [per_device(): down_whole = jnp.concatenate(lax.all_gather(w_down, SP), axis=1)]
    all_gather x2, blocking collectives: 53.6 us -> 49.7 us  [all_in_one(): both, at, found = (lax.all_gather(jnp.concatenate(lines), axis), 0, {})]
    all_to_all x0 -> x1, starting transfers between devices: none -> 3.79 us  [sent_to_all(): lax.all_to_all(jnp.broadcast_to(shard[None], (count, *shard.shape)), axis...]
    unnamed x12 -> x13, local copies, waits for them, and re-layouts: 0.99 us -> 4.71 us
  transfers between devices with their start and end apart: 3 -> 4, of which waited for: 2 -> 2; matrix products, arithmetic and copies ran while one was open for 31% -> 33% of each run, Pallas kernels for 0% -> 0%
where the time goes in v1:
time: 212 us; the launch traced here: 210 us
  blocking collectives  62.5 us (29%)
  waiting for transfers between devices  44.5 us (21%)
  local copies, waits for them, and re-layouts  33.7 us (16%)
  other arithmetic  26.8 us (13%)
  matrix products  21.4 us (10%)
  between operations  13.7 us (6%)
  starting transfers between devices  7.66 us (4%)
    all_gather x2, blocking collectives, all_in_one(): both, at, found = (lax.all_gather(jnp.concatenate(lines), axis), 0, {})  49.7 us
    all_gather x1, waiting for transfers between devices, sent_together(): lax.all_gather(both, axis, axis=dim, tiled=True)  39.1 us
    all_to_all x1, blocking collectives, summed_on_arrival(): lax.all_to_all(pieces, axis, split_axis=0, concat_axis=0, tiled=True)  12.8 us
    dynamic_update_slice x16, local copies, waits for them, and re-layouts, local_states(): lax.scan(carry_step, (zeros, zeros), (inner_re[:, -1], inner_im[:, -1]))  12.1 us
    dot_general x1, matrix products, per_device(): jnp.dot(hidden, down_whole, preferred_element_type=jnp.float32)  7.42 us
    add x1, other arithmetic, per_device(): state_im = local_im + pow_re * carried[3][None] + pow_im * carried[2][None]  6.71 us
    reduce_sum x1, other arithmetic, local_states(): jnp.sum(table_re[None] * block_im + table_im[None] * block_re, axis=2)  6.2 us
    unnamed x13, local copies, waits for them, and re-layouts  4.71 us
  transfers between devices with their start and end apart: 4, of which 2 were waited for; matrix products, arithmetic and copies ran while one was open for 33% of the time, Pallas kernels for 0%

profile of v1, /device:TPU:33, one launch (start us, length us, event | category | flops | bytes accessed | tf_op | source)
XLA Modules:
  0.0 210.5 jit_solution(13554760460877968577)
XLA Ops:
  7.4 1.8 pad_maximum_fusion
  11.7 2.0 convolution_bitcast_fusion
  13.8 1.5 copy.55
  16.6 2.1 convolution_bitcast_fusion.1
  18.6 1.5 copy.54
  21.7 4.0 %fusion.19 = (f32[16,16,1024]{2,1,0:T(8,128)S(1)}, f32[16,16,1024]{2,1,0:T(8,128)S(1)}) fusion(f32[1024]{0:T(1024)S(1)} %mul.861, f32[16,16]{1,0:T(8,128)S(1)} %convert_maximum_fusion, f32[1024]{0:T(1024)S(1)} %mul.856, pred[16,16]{1,0:T(8,128)(4,1)S(1)} %iota_compare_fusion), kind=kLoop, calls=%fused_computation.33 | loop fusion | flops 1572864 | bytes 2106624 | tf_op jit(solution)/shard_map/jit(_where)/select_n | solution.py:143
  25.7 6.2 %add_reduce_fusion = (f32[8,16,1024]{2,1,0:T(8,128)S(1)}, f32[8,16,1024]{2,1,0:T(8,128)S(1)}) fusion(f32[8,16,1024]{2,1,0:T(8,128)} %mul.885, f32[16,16,1024]{2,1,0:T(8,128)S(1)} %get-tuple-element.125, f32[8,16,1024]{2,1,0:T(8,128)} %mul.878, f32[16,16,1024]{2,1,0:T(8,128)S(1)} %get-tuple-element.124), kind=kLoop, calls=%fused_computation.6 | loop fusion | flops 16515072 | bytes 4194304 | tf_op jit(solution)/shard_map/reduce_sum | solution.py:148
  32.0 12.5 %while.17 = (s32[]{:T(128)}, f32[1024]{0:T(1024)S(1)}, f32[1024]{0:T(1024)S(1)}, f32[8,1024]{1,0:T(8,128)S(1)}, f32[8,1024]{1,0:T(8,128)}, /*index=5*/f32[1024]{...) while((s32[]{:T(128)}, f32[1024]{0:T(1024)S(1)}, ...), condition=%wide.region_3.4_spmd.clone, body=%wide.region_2.3_spmd.clone.sunk | while | flops 10243 | bytes 90251 | solution.py:162
  44.5 1.9 multiply_add_fusion.1
  47.8 2.3 %sub.173 = f32[128,16,64]{2,1,0:T(8,128)} reshape(f32[8,16,1024]{2,1,0:T(8,128)} %get-tuple-element.118) | data formatting | bytes 1048576 | tf_op jit(solution)/shard_map/sub | solution.py:165
  50.9 3.9 %fusion.22 = (f32[128,16,64]{2,1,0:T(8,128)S(1)}, f32[128,16,64]{2,1,0:T(8,128)S(1)}) fusion(f32[16,64]{1,0:T(8,128)S(1)} %get-tuple-element.133, f32[128]{0:T(128)S(1)} %add_convert_fusion.1, f32[16,64]{1,0:T(8,128)S(1)} %get-tuple-element.132), kind=kLoop, calls=%fused_computation.36 | loop fusion | flops 524288 | bytes 1057280 | tf_op jit(solution)/shard_map/mul | solution.py:109
  54.8 22.0 %all-gather = f32[128,64]{1,0:T(8,128)S(1)} all-gather(f32[64,64]{1,0:T(8,128)S(1)} %pad_maximum_fusion.1), channel_id=2, replica_groups=mesh['grp'=2,'sp_0'=16,'sp_1'=2,'tp'=4] {'sp_1'}, dimensions={0}, use_global_device_ids=true | all-gather | bytes 49152 | tf_op jit(solution)/shard_map/all_gather | solution.py:37
  76.8 27.8 %all-gather.1 = f32[1024,64]{1,0:T(8,128)S(1)} all-gather(f32[64,64]{1,0:T(8,128)S(1)} %pad_maximum_fusion.2), channel_id=3, replica_groups=mesh['grp'=2,'sp_0'=16,'sp_1'=2,'tp'=4] {'sp_0'}, dimensions={0}, use_global_device_ids=true | all-gather | bytes 278528 | tf_op jit(solution)/shard_map/all_gather | solution.py:37
  104.7 6.7 %multiply_add_fusion = (bf16[128,16,64]{2,1,0:T(8,128)(2,1)S(1)}, bf16[128,16,64]{2,1,0:T(8,128)(2,1)S(1)}) fusion(f32[128,16,64]{2,1,0:T(8,128)S(1)} %add.447, f32[16,64]{1,0:T(8,128)S(1)} %add_bitcast_fusion, f32[16,64]{1,0:T(8,128)S(1)} %get-tuple-element.108, f32[16,64]{1,0:T(8,128)S(1)} %get-tuple-element.133, f32[128]{0:T(128)S(1)} %add_convert_fusion.1, ...), kind=kLoop, calls=%fused_computation.42 | loop fusion | flops 1835008 | bytes 1589760 | tf_op jit(solution)/shard_map/add | solution.py:229
  114.1 3.8 %all-to-all-start = ((bf16[4,32,256]{2,1,0:T(8,128)(2,1)}), bf16[4,32,256]{2,1,0:T(8,128)(2,1)S(1)}, u32[]{:S(2)}, u32[]{:S(2)}) async-start(bf16[4,32,256]{2,1,0:T(8,128)(2,1)} %copy.58), calls=%async_computation | async-start | bytes 131072 | tf_op jit(solution)/shard_map/all_to_all | solution.py:233
  117.9 4.5 %all-to-all-done = bf16[4,32,256]{2,1,0:T(8,128)(2,1)S(1)} async-done(((bf16[4,32,256]{2,1,0:T(8,128)(2,1)}), bf16[4,32,256]{2,1,0:T(8,128)(2,1)S(1)}, u32[]{:S(2)}, u32[]{:S(2)}) %all-to-all-start) | async-done | bytes 65568 | tf_op jit(solution)/shard_map/all_to_all | solution.py:233
  122.4 3.6 %multiply_reduce_fusion = (f32[32]{0:T(128)S(1)}, f32[32,2048]{1,0:T(8,128)S(1)}) fusion(bf16[1024,2048]{1,0:T(8,128)(2,1)} %param.31, bf16[32,1024]{1,0:T(8,128)(2,1)S(1)} %bitcast.184, bf16[1024,1024]{1,0:T(8,128)(2,1)S(1)} %copy-done, f32[1024]{0:T(1024)S(1)} %copy-done.3, bf16[128,2048]{1,0:T(8,128)(2,1)} %param.20, s32[]{:T(128)S(6)} %select_n.296), kind=kOutput, calls=%fused_computation.57 | convolution fusion | flops 201818080 | bytes 6819972 | tf_op jit(solution)/shard_map/dot_general | solution.py:237
  127.0 3.8 %all-to-all-start.1 = ((bf16[4,32,2048]{2,1,0:T(8,128)(2,1)}), bf16[4,32,2048]{2,1,0:T(8,128)(2,1)S(1)}, u32[]{:S(2)}, u32[]{:S(2)}) async-start(bf16[4,32,2048]{2,1,0:T(8,128)(2,1)} %broadcast_in_dim.32), calls=%async_computation.1 | async-start | bytes 1048576 | tf_op jit(solution)/shard_map/all_to_all | solution.py:63
  130.9 3.7 %copy.64 = bf16[8,8,32,1408]{3,2,1,0:T(8,128)(2,1)S(1)} copy(bf16[8,8,32,1408]{3,1,2,0:T(8,128)(2,1)} %bitcast.166) | data formatting | bytes 11534336
  134.6 4.5 %copy.60 = bf16[1408,32,64]{0,2,1:T(8,128)(2,1)} copy(bf16[1408,32,64]{0,1,2:T(8,128)(2,1)S(1)} %bitcast.165) | data formatting | bytes 11534336 | tf_op jit(solution)/shard_map/reshape | solution.py:245
  139.0 39.1 %all-gather.6.cloned.1.call-done = bf16[2048,2816]{1,0:T(8,128)(2,1)} async-done(((bf16[64,2816]{1,0:T(8,128)(2,1)}), bf16[2048,2816]{1,0:T(8,128)(2,1)}) %all-gather.6.cloned.1.call-update) | async-done | bytes 11534352 | tf_op jit(solution)/shard_map/all_gather | solution.py:20
  178.2 4.5 %fusion.2 = f32[128,1408]{1,0:T(8,128)} fusion(bf16[128,2048]{1,0:T(8,128)(2,1)S(1)} %bitcast.177, bf16[2048,2816]{1,0:T(8,128)(2,1)} %all-gather.6.cloned.1.call-done), kind=kOutput, calls=%fused_computation.10 | convolution fusion | flops 738197504 | bytes 7012352 | tf_op jit(solution)/shard_map/dot_general | solution.py:242
  182.7 7.4 %convolution_convert_fusion = bf16[128,2048]{1,0:T(8,128)(2,1)S(1)} fusion(bf16[1408,2048]{0,1:T(8,128)(2,1)} %bitcast.167, bf16[128,2048]{1,0:T(8,128)(2,1)S(1)} %bitcast.178, bf16[2048,2816]{1,0:T(8,128)(2,1)} %all-gather.6.cloned.1.call-done, f32[128,1408]{1,0:T(8,128)} %fusion.2), kind=kOutput, calls=%fused_computation.14 | convolution fusion | flops 1477738496 | bytes 13303808 | tf_op jit(solution)/shard_map/dot_general | solution.py:247
  190.1 12.8 %all_to_all.26 = bf16[4,32,2048]{2,1,0:T(8,128)(2,1)S(1)} all-to-all(bf16[4,32,2048]{2,1,0:T(8,128)(2,1)S(1)} %bitcast.179), channel_id=1, replica_groups=mesh['grp'=2,'sp_0'=16,'sp_1'=2,'tp'=4] {'tp'}, dimensions={0} | all-to-all | bytes 1048576 | tf_op jit(solution)/shard_map/all_to_all | solution.py:87
  (98 shorter events, 25.1 us)
Async XLA Ops:
  6.5 115.9 %copy-start = (bf16[1024,1024]{1,0:T(8,128)(2,1)S(1)}, bf16[1024,1024]{1,0:T(8,128)(2,1)}, u32[]{:S(2)}) copy-start(bf16[1024,1024]{1,0:T(8,128)(2,1)} %param.29) | copy-start | bytes 6291460
  6.6 124.3 %all-gather.8.cloned.1.call-start = ((), (), s32[]{:S(2)}) async-start(), calls=%async_computation.4 | async-start | bytes 5947392 | tf_op jit(solution)/shard_map/all_gather | solution.py:245
  7.3 170.8 %all-gather.6.cloned.1.call-start = ((), (), s32[]{:S(2)}) async-start(), calls=%async_computation.3 | async-start | bytes 11894784 | tf_op jit(solution)/shard_map/all_gather | solution.py:20
  25.7 24.4 %copy-start.4 = (f32[256]{0:T(256)S(1)}, f32[256]{0:T(256)}, u32[]{:S(2)}) copy-start(f32[256]{0:T(256)} %param.28) | copy-start | bytes 3076
  44.5 66.9 %copy-start.1 = (f32[16,16,64]{2,1,0:T(8,128)S(1)}, f32[16,16,64]{2,1,0:T(8,128)}, u32[]{:S(2)}) copy-start(f32[16,16,64]{2,1,0:T(8,128)} %param.26) | copy-start | bytes 196612
  47.8 74.7 %copy-start.3 = (f32[1024]{0:T(1024)S(1)}, f32[1024]{0:T(1024)}, u32[]{:S(2)}) copy-start(f32[1024]{0:T(1024)} %param.30) | copy-start | bytes 12292
  104.7 21.4 %copy-start.2 = (f32[2048]{0:T(1024)S(1)}, f32[2048]{0:T(1024)}, u32[]{:S(2)}) copy-start(f32[2048]{0:T(1024)} %param.32) | copy-start | bytes 24580
  114.1 8.3 %all-to-all-start = ((bf16[4,32,256]{2,1,0:T(8,128)(2,1)}), bf16[4,32,256]{2,1,0:T(8,128)(2,1)S(1)}, u32[]{:S(2)}, u32[]{:S(2)}) async-start(bf16[4,32,256]{2,1,0:T(8,128)(2,1)} %copy.58), calls=%async_computation | async-start | bytes 131072 | tf_op jit(solution)/shard_map/all_to_all | solution.py:233
  127.0 12.0 %all-to-all-start.1 = ((bf16[4,32,2048]{2,1,0:T(8,128)(2,1)}), bf16[4,32,2048]{2,1,0:T(8,128)(2,1)S(1)}, u32[]{:S(2)}, u32[]{:S(2)}) async-start(bf16[4,32,2048]{2,1,0:T(8,128)(2,1)} %broadcast_in_dim.32), calls=%async_computation.1 | async-start | bytes 1048576 | tf_op jit(solution)/shard_map/all_to_all | solution.py:63
Sparse Core Ops, SparseCore 0:
  9.2 89.1 all-gather.7
  100.2 77.8 all-gather.5
